TPU v7x, 32 devices: a whole 2x2x4 slice. The times are simulated.
32 devices in a mesh: kv: 8 (over z, y), tp: 4 (over x, core).
Axes of the slice: x: 2, y: 2, z: 4, core: 2. Of those that a mesh axis runs over, the one named last changes fastest.
Arguments:
- tokens: bfloat16 [256, 4096], P(None, ('kv', 'tp')), may hold values from -60 to 60
- past_state: float32 [256, 16, 128, 128], P('kv', 'tp'), may hold values from -4 to 4
- pre_gain: float32 [4096], replicated, may hold values from 0.1 to 1.9
- pre_gate: bfloat16 [4096, 11264], P(None, ('kv', 'tp')), may hold values from -0.09375 to 0.09375
- pre_up: bfloat16 [4096, 11264], P(None, ('kv', 'tp')), may hold values from -0.09375 to 0.09375
- pre_down: bfloat16 [11264, 4096], P(('kv', 'tp')), may hold values from -0.109375 to 0.109375
- mix_gain: float32 [4096], replicated, may hold values from 0.1 to 1.9
- query_weight: bfloat16 [4096, 2048], P('kv', 'tp'), may hold values from -0.09375 to 0.09375
- forget_weight: bfloat16 [4096, 2048], P('kv', 'tp'), may hold values from -0.09375 to 0.09375
- value_weight: bfloat16 [4096, 2048], P('kv', 'tp'), may hold values from -0.09375 to 0.09375
- output_gate_weight: bfloat16 [4096, 2048], P('kv', 'tp'), may hold values from -0.09375 to 0.09375
- forget_floor: float32 [2048], P('tp'), may hold values from 0.02 to 0.9
- head_gain: float32 [128], replicated, may hold values from 0.1 to 1.9
- proj_out: bfloat16 [2048, 4096], P('tp', 'kv'), may hold values from -0.125 to 0.125
- post_gain: float32 [4096], replicated, may hold values from 0.1 to 1.9
- post_gate: bfloat16 [4096, 11264], P(None, ('kv', 'tp')), may hold values from -0.09375 to 0.09375
- post_up: bfloat16 [4096, 11264], P(None, ('kv', 'tp')), may hold values from -0.09375 to 0.09375
- post_down: bfloat16 [11264, 4096], P(('kv', 'tp')), may hold values from -0.109375 to 0.109375
Outputs:
- result: bfloat16 [256, 4096], P(None, ('kv', 'tp'))
- new_state: float32 [256, 16, 128, 128], P('kv', 'tp')
All inputs are finite; a program needn't handle non-finite values.
Results may differ from a plain program's by a relative error of at most 0.014.
Values may be sent and summed in bfloat16 or wider, within the bound.
A program may use at most 128 MiB of HBM per device.

v0:
```python
import jax
import jax.numpy as jnp
from jax import lax
from jax.sharding import PartitionSpec as P

D = 4096
epsilon = 1e-06


def half_inputs(activations, gain, w_gate, w_up):
    piece_float = lax.all_gather(activations, ("kv", "tp"), axis=1, tiled=True).astype(jnp.float32)
    normed = (piece_float * gain).astype(jnp.bfloat16)
    gate_acc = jnp.dot(normed, w_gate, preferred_element_type=jnp.float32)
    up_acc = jnp.dot(normed, w_up, preferred_element_type=jnp.float32)
    squares = jnp.sum(piece_float * piece_float, axis=1)
    row_scale = lax.rsqrt(squares / D + epsilon)[:, None]
    return (jax.nn.silu(row_scale * gate_acc) * (row_scale * up_acc)).astype(jnp.bfloat16)


def down_sum(hidden, w_down):
    return lax.psum_scatter(
        jnp.dot(hidden, w_down, preferred_element_type=jnp.float32),
        ("kv", "tp"),
        scatter_dimension=1,
        tiled=True,
    )


def per_device(
    tokens,
    past_state,
    pre_gain,
    pre_gate,
    pre_up,
    pre_down,
    mix_gain,
    query_weight,
    forget_weight,
    value_weight,
    output_gate_weight,
    forget_floor,
    head_gain,
    proj_out,
    post_gain,
    post_gate,
    post_up,
    post_down,
):
    whole_rows = lax.all_gather(tokens, ("kv", "tp"), axis=1, tiled=True)
    whole_float = whole_rows.astype(jnp.float32)
    row_scale = lax.rsqrt(jnp.mean(whole_float * whole_float, axis=1, keepdims=True) + epsilon)
    normed = (whole_float * pre_gain).astype(jnp.bfloat16)
    gate_pre = row_scale * jnp.dot(normed, pre_gate, preferred_element_type=jnp.float32)
    up_pre = row_scale * jnp.dot(normed, pre_up, preferred_element_type=jnp.float32)
    hidden = (jax.nn.silu(gate_pre) * up_pre).astype(jnp.bfloat16)
    kv_sums = lax.psum_scatter(
        jnp.dot(hidden, pre_down, preferred_element_type=jnp.float32).astype(jnp.bfloat16),
        "kv",
        scatter_dimension=1,
        tiled=True,
    )
    block_sum = lax.psum(kv_sums, "tp").astype(jnp.float32)
    block_width = block_sum.shape[1]
    block_old = lax.dynamic_slice_in_dim(
        whole_rows, lax.axis_index("kv") * block_width, block_width, 1
    )
    block_rows = (block_old.astype(jnp.float32) + 0.5 * block_sum).astype(jnp.bfloat16)
    own_width = block_width // lax.axis_size("tp")
    after_first = lax.dynamic_slice_in_dim(
        block_rows, lax.axis_index("tp") * own_width, own_width, 1
    )
    block_width = block_rows.shape[1]
    block_float = block_rows.astype(jnp.float32)
    block_gain = lax.dynamic_slice_in_dim(
        mix_gain, lax.axis_index("kv") * block_width, block_width, 0
    )
    squares = lax.psum(jnp.sum(block_float * block_float, axis=1), "kv")
    normed = (block_float * block_gain).astype(jnp.bfloat16)
    own_rows = past_state.shape[0]
    weight_list = (query_weight, forget_weight, value_weight, output_gate_weight)
    projected = lax.psum_scatter(
        jnp.concatenate(
            [
                jnp.dot(normed, weight_part, preferred_element_type=jnp.float32)
                for weight_part in weight_list
            ],
            axis=1,
        ).astype(jnp.bfloat16),
        "kv",
        scatter_dimension=0,
        tiled=True,
    ).astype(jnp.float32)
    own_squares = lax.dynamic_slice_in_dim(squares, lax.axis_index("kv") * own_rows, own_rows, 0)
    projected = projected * lax.rsqrt(own_squares / D + epsilon)[:, None]
    pre_query, pre_forget, pre_value, pre_gate_out = jnp.split(projected, 4, axis=1)
    local_heads = past_state.shape[1]
    head_width = past_state.shape[2]
    head_shape = (own_rows, local_heads, head_width)
    floors = forget_floor.reshape(local_heads, head_width)
    forget_heads = pre_forget.reshape(head_shape)
    forget = floors + (1.0 - floors) * jax.nn.sigmoid(forget_heads)
    written = (1.0 - floors) * jax.nn.sigmoid(-forget_heads)
    query_act = jax.nn.silu(pre_query.reshape(head_shape))
    value_act = pre_value.reshape(head_shape)
    new_state = (
        forget[:, :, :, None] * past_state + written[:, :, :, None] * value_act[:, :, None, :]
    )
    readout = jnp.einsum("bhkv,bhk->bhv", new_state, query_act, precision=lax.Precision.HIGHEST)
    readout = (
        readout
        * lax.rsqrt(jnp.mean(readout * readout, axis=2, keepdims=True) + epsilon)
        * head_gain
    )
    mixed_in = (
        readout.reshape(own_rows, local_heads * head_width) * jax.nn.silu(pre_gate_out)
    ).astype(jnp.bfloat16)
    partials = jnp.dot(
        lax.all_gather(mixed_in, "kv", axis=0, tiled=True),
        proj_out,
        preferred_element_type=jnp.float32,
    ).astype(jnp.bfloat16)
    mixed_sum = lax.psum_scatter(partials, "tp", scatter_dimension=1, tiled=True).astype(
        jnp.float32
    )
    second = (after_first.astype(jnp.float32) + mixed_sum).astype(jnp.bfloat16)
    hidden_two = half_inputs(second, post_gain, post_gate, post_up)
    result = (second.astype(jnp.float32) + 0.5 * down_sum(hidden_two, post_down)).astype(
        jnp.bfloat16
    )
    return (result, new_state)


def solution(mesh):
    placed = (
        P(None, ("kv", "tp")),
        P("kv", "tp", None, None),
        P(),
        P(None, ("kv", "tp")),
        P(None, ("kv", "tp")),
        P(("kv", "tp"), None),
        P(),
        P("kv", "tp"),
        P("kv", "tp"),
        P("kv", "tp"),
        P("kv", "tp"),
        P("tp"),
        P(),
        P("tp", "kv"),
        P(),
        P(None, ("kv", "tp")),
        P(None, ("kv", "tp")),
        P(("kv", "tp"), None),
    )
    return jax.shard_map(
        per_device,
        mesh=mesh,
        in_specs=placed,
        out_specs=(P(None, ("kv", "tp")), P("kv", "tp", None, None)),
        check_vma=False,
    )
```

profile of v0, /device:TPU:0, one launch (start us, length us, event | category | flops | bytes accessed | tf_op | source)
XLA Modules:
  0.0 548.7 jit_solution(15226853268982632663)
XLA Ops:
  8.0 58.6 %all-gather.3.cloned.1.call-done = bf16[256,4096]{1,0:T(8,128)(2,1)} async-done(((bf16[256,128]{1,0:T(8,128)(2,1)}), bf16[256,4096]{1,0:T(8,128)(2,1)}) %all-gather.3.cloned.1.call-update) | async-done | bytes 2097168 | tf_op jit(solution)/shard_map/all_gather | solution.py:49
  66.6 2.1 fusion
  68.7 3.4 fusion.12
  72.1 7.5 %convolution_convert_fusion = bf16[256,4096]{1,0:T(8,128)(2,1)} fusion(bf16[352,4096]{1,0:T(8,128)(2,1)S(1)} %copy-done, bf16[4096,352]{0,1:T(8,128)(2,1)} %param.22, bf16[256,4096]{1,0:T(8,128)(2,1)} %all-gather.3.cloned.1.call-done, f32[4096]{0:T(1024)S(1)} %copy-done.7, f32[256,352]{0,1:T(8,128)S(1)} %fusion.12, f32[256]{0:T(256)S(1)} %add_rsqrt_fusion.2), kind=kOutput, calls=%fused_computation.5 | convolution fusion | flops 1481220096 | bytes 10339328 | tf_op jit(solution)/shard_map/dot_general | solution.py:57
  79.7 68.1 %reduce-scatter.7.cloned.1.call-done = bf16[256,512]{1,0:T(8,128)(2,1)} async-done(((bf16[256,4096]{1,0:T(8,128)(2,1)}), bf16[256,512]{1,0:T(8,128)(2,1)}) %reduce-scatter.7.cloned.1.call-update) | async-done | bytes 262160 | tf_op jit(solution)/shard_map/reduce_scatter | solution.py:56
  148.6 32.8 %all-reduce.2.cloned.1.call-done = bf16[256,512]{1,0:T(8,128)(2,1)} async-done(((bf16[256,512]{1,0:T(8,128)(2,1)}), bf16[256,512]{1,0:T(8,128)(2,1)}) %all-reduce.2.cloned.1.call-update) | async-done | bytes 262160 | tf_op jit(solution)/shard_map/psum | solution.py:62
  181.4 1.2 fusion.42
  182.6 1.3 convolution_convert_fusion.3
  183.9 1.3 convolution_convert_fusion.2
  185.3 1.3 convolution_convert_fusion.4
  186.6 1.3 convolution_convert_fusion.5
  189.2 21.6 %psum.15 = f32[256]{0:T(256)S(1)} all-reduce(f32[256]{0:T(256)S(1)} %get-tuple-element.2), channel_id=1, replica_groups=mesh['kv'=8,'tp'=4] {'kv'}, use_global_device_ids=true, to_apply=%region_5.6 | all-reduce | flops 256 | bytes 2048 | tf_op jit(solution)/shard_map/psum | solution.py:77
  210.8 42.6 %reduce-scatter.9.cloned.1.call-done = bf16[32,2048]{1,0:T(8,128)(2,1)} async-done(((bf16[256,2048]{1,0:T(8,128)(2,1)}), bf16[32,2048]{1,0:T(8,128)(2,1)}) %reduce-scatter.9.cloned.1.call-update) | async-done | bytes 131088 | tf_op jit(solution)/shard_map/reduce_scatter | solution.py:81
  258.2 1.5 div.63
  260.5 8.2 %multiply_add_fusion = f32[32,4,128,128]{3,2,1,0:T(8,128)S(1)} fusion(f32[32,4,128,128]{3,2,1,0:T(8,128)} %param.19, f32[32,4,128]{2,1,0:T(4,128)S(1)} %mul.203, f32[32,4,128]{2,1,0:T(4,128)S(1)} %bitcast.39, f32[32,4,128]{2,1,0:T(4,128)S(1)} %bitcast.38), kind=kLoop, calls=%fused_computation | loop fusion | flops 6291456 | bytes 16973824 | tf_op jit(solution)/shard_map/add | solution.py:106
  268.8 7.2 %fusion.65 = f32[32,4,1,128]{3,2,1,0:T(1,128)S(1)} fusion(f32[32,4,128,128]{3,2,1,0:T(8,128)S(1)} %multiply_add_fusion, f32[32,4,128,1]{2,3,1,0:T(1,128)S(1)} %bitcast.37), kind=kOutput, calls=%fused_computation.68 | convolution fusion | flops 25165824 | bytes 8519680 | tf_op jit(solution)/shard_map/bhkv,bhk->bhv/dot_general | solution.py:108
  276.3 30.8 %all_gather.10 = bf16[256,512]{1,0:T(8,128)(2,1)S(1)} all-gather(bf16[32,512]{1,0:T(8,128)(2,1)S(1)} %fusion.61), channel_id=1, replica_groups=mesh['kv'=8,'tp'=4] {'kv'}, dimensions={0}, use_global_device_ids=true | all-gather | bytes 294912 | tf_op jit(solution)/shard_map/all_gather | solution.py:118
  308.3 19.2 %reduce-scatter.13.cloned.1.call-done = bf16[128,256]{1,0:T(8,128)(2,1)} async-done(((bf16[512,256]{1,0:T(8,128)(2,1)}), bf16[128,256]{1,0:T(8,128)(2,1)}) %reduce-scatter.13.cloned.1.call-update) | async-done | bytes 65552
  329.4 54.4 %all-gather.5.cloned.1.call-done = bf16[256,4096]{1,0:T(8,128)(2,1)} async-done(((bf16[256,128]{1,0:T(8,128)(2,1)}), bf16[256,4096]{1,0:T(8,128)(2,1)}) %all-gather.5.cloned.1.call-update) | async-done | bytes 2097168 | tf_op jit(solution)/shard_map/all_gather | solution.py:11
  383.8 2.1 fusion.2
  385.9 3.4 fusion.18
  389.3 8.9 %fusion.37 = f32[256,4096]{1,0:T(8,128)} fusion(bf16[352,4096]{1,0:T(8,128)(2,1)} %param.35, bf16[4096,352]{0,1:T(8,128)(2,1)} %param.34, bf16[256,4096]{1,0:T(8,128)(2,1)} %all-gather.5.cloned.1.call-done, f32[4096]{0:T(1024)S(1)} %copy-done.4, f32[256,352]{0,1:T(8,128)S(1)} %fusion.18, f32[256]{0:T(256)S(1)} %add_rsqrt_fusion.1), kind=kOutput, calls=%fused_computation.27 | convolution fusion | flops 1480171520 | bytes 12436480 | tf_op jit(solution)/shard_map/dot_general | solution.py:22
  398.3 142.1 %reduce-scatter.11.cloned.1.call-done = f32[256,128]{1,0:T(8,128)} async-done(((f32[256,4096]{1,0:T(8,128)}), f32[256,128]{1,0:T(8,128)}) %reduce-scatter.11.cloned.1.call-update) | async-done | bytes 131088 | tf_op jit(solution)/shard_map/reduce_scatter | solution.py:21
  540.3 1.6 add_convert_fusion.1
  (53 shorter events, 11.8 us)
Async XLA Ops:
  7.2 65.0 %copy-start = (bf16[352,4096]{1,0:T(8,128)(2,1)S(1)}, bf16[352,4096]{1,0:T(8,128)(2,1)}, u32[]{:S(2)}) copy-start(bf16[352,4096]{1,0:T(8,128)(2,1)} %param.23) | copy-start | bytes 8650756
  7.2 59.4 %all-gather.3.cloned.1.call-start = ((), (), s32[]{:S(2)}) async-start(), calls=%async_computation.4 | async-start | bytes 2162688 | tf_op jit(solution)/shard_map/all_gather | solution.py:49
  7.9 139.8 %reduce-scatter.7.cloned.1.call-start = ((), (), s32[]{:S(2)}) async-start(), calls=%async_computation.5 | async-start | bytes 2359296 | tf_op jit(solution)/shard_map/reduce_scatter | solution.py:56
  68.7 3.5 copy-start.7
  79.6 101.7 %all-reduce.2.cloned.1.call-start = ((), (), s32[]{:S(2)}) async-start(), calls=%async_computation.6 | async-start | bytes 524288 | tf_op jit(solution)/shard_map/psum | solution.py:62
  147.8 105.7 %reduce-scatter.9.cloned.1.call-start = ((), (), s32[]{:S(2)}) async-start(), calls=%async_computation.7 | async-start | bytes 1179648 | tf_op jit(solution)/shard_map/reduce_scatter | solution.py:81
  185.3 3.9 copy-start.5
  189.1 138.4 %reduce-scatter.13.cloned.1.call-start = ((), (), s32[]{:S(2)}) async-start(), calls=%async_computation.10 | async-start | bytes 327680
  268.8 7.2 %copy-start.1 = (f32[32,4,128,128]{3,2,1,0:T(8,128)}, f32[32,4,128,128]{3,2,1,0:T(8,128)S(1)}, u32[]{:S(2)}) copy-start(f32[32,4,128,128]{3,2,1,0:T(8,128)S(1)} %multiply_add_fusion) | copy-start | bytes 25165828
  268.8 7.3 %copy-start.6 = (f32[128]{0:T(128)S(1)}, f32[128]{0:T(128)}, u32[]{:S(2)}) copy-start(f32[128]{0:T(128)} %param.30) | copy-start | bytes 1540
  268.8 38.3 %copy-start.3 = (bf16[512,512]{1,0:T(8,128)(2,1)S(1)}, bf16[512,512]{1,0:T(8,128)(2,1)}, u32[]{:S(2)}) copy-start(bf16[512,512]{1,0:T(8,128)(2,1)} %param.31) | copy-start | bytes 1572868
  276.0 109.9 %copy-start.4 = (f32[4096]{0:T(1024)S(1)}, f32[4096]{0:T(1024)}, u32[]{:S(2)}) copy-start(f32[4096]{0:T(1024)} %param.32) | copy-start | bytes 49156
  308.3 75.5 %all-gather.5.cloned.1.call-start = ((), (), s32[]{:S(2)}) async-start(), calls=%async_computation.8 | async-start | bytes 2162688 | tf_op jit(solution)/shard_map/all_gather | solution.py:11
  329.1 211.2 %reduce-scatter.11.cloned.1.call-start = ((), (), s32[]{:S(2)}) async-start(), calls=%async_computation.9 | async-start | bytes 4325376 | tf_op jit(solution)/shard_map/reduce_scatter | solution.py:21
  398.2 142.1 %copy-start.2 = (bf16[256,128]{1,0:T(8,128)(2,1)S(1)}, bf16[256,128]{1,0:T(8,128)(2,1)}, u32[]{:S(2)}) copy-start(bf16[256,128]{1,0:T(8,128)(2,1)} %add_convert_fusion.2) | copy-start | bytes 196612
Sparse Core Ops, SparseCore 0:
  10.8 55.6 all-gather.2
  79.7 67.9 reduce-scatter.6
  150.1 31.2 all-reduce.1
  189.2 64.1 reduce-scatter.8
  308.4 19.0 reduce-scatter.12
  330.8 52.9 all-gather.4
  398.4 141.8 reduce-scatter.10
where the time goes:
time: 550 us; the launch traced here: 549 us
  waiting for transfers between devices  418 us (76%)
  blocking collectives  52.4 us (10%)
  matrix products  36.1 us (7%)
  other arithmetic  20.7 us (4%)
  between operations  14.4 us (3%)
  local copies, waits for them, and re-layouts  6.21 us (1%)
    reduce_scatter x1, waiting for transfers between devices, down_sum(): lax.psum_scatter(jnp.dot(hidden, w_down, preferred_element_type=jnp.float...  142 us
    reduce_scatter x1, waiting for transfers between devices, per_device(): lax.psum_scatter(jnp.dot(hidden, pre_down, preferred_element_type=jnp.flo...  68.1 us
    all_gather x1, waiting for transfers between devices, per_device(): whole_rows = lax.all_gather(tokens, ('kv', 'tp'), axis=1, tiled=True)  58.6 us
    all_gather x1, waiting for transfers between devices, half_inputs(): lax.all_gather(activations, ('kv', 'tp'), axis=1, tiled=True)  54.4 us
    reduce_scatter x1, waiting for transfers between devices, per_device(): lax.psum_scatter(jnp.concatenate([jnp.dot(normed, weight_part, preferred_...  42.6 us
    psum x1, waiting for transfers between devices, per_device(): block_sum = lax.psum(kv_sums, 'tp').astype(jnp.float32)  32.8 us
    all_gather x1, blocking collectives, per_device(): lax.all_gather(mixed_in, 'kv', axis=0, tiled=True)  30.8 us
    psum x1, blocking collectives, per_device(): squares = lax.psum(jnp.sum(block_float * block_float, axis=1), 'kv')  21.6 us
  transfers between devices with their start and end apart: 7, of which 7 were waited for; matrix products, arithmetic and copies ran while one was open for 0% of the time, Pallas kernels for 0%

commit v1 on v0

--- a/solution.py
+++ b/solution.py
@@ -5,6 +5,11 @@
 
 D = 4096
 epsilon = 1e-06
+
+
+def summed_here(array, name):
+    parts = lax.all_gather(array, name)
+    return jnp.sum(parts, axis=0)
 
 
 def half_inputs(activations, gain, w_gate, w_up):
@@ -59,7 +64,7 @@
         scatter_dimension=1,
         tiled=True,
     )
-    block_sum = lax.psum(kv_sums, "tp").astype(jnp.float32)
+    block_sum = summed_here(kv_sums, "tp").astype(jnp.float32)
     block_width = block_sum.shape[1]
     block_old = lax.dynamic_slice_in_dim(
         whole_rows, lax.axis_index("kv") * block_width, block_width, 1

time: 550 us -> 532 us (0.967)
  waiting for transfers between devices: 418 us -> 402 us
    psum x1 -> x0, waiting for transfers between devices: 32.8 us -> none  [per_device(): block_sum = lax.psum(kv_sums, 'tp').astype(jnp.float32)]
    all_gather x0 -> x1, waiting for transfers between devices: none -> 16.4 us  [summed_here(): parts = lax.all_gather(array, name)]
where the time goes in v1:
time: 532 us; the launch traced here: 531 us
  waiting for transfers between devices  402 us (76%)
  blocking collectives  52.4 us (10%)
  matrix products  34 us (6%)
  other arithmetic  22.2 us (4%)
  between operations  14.4 us (3%)
  local copies, waits for them, and re-layouts  6.24 us (1%)
    reduce_scatter x1, waiting for transfers between devices, down_sum(): lax.psum_scatter(jnp.dot(hidden, w_down, preferred_element_type=jnp.float...  142 us
    reduce_scatter x1, waiting for transfers between devices, per_device(): lax.psum_scatter(jnp.dot(hidden, pre_down, preferred_element_type=jnp.flo...  68.1 us
    all_gather x1, waiting for transfers between devices, per_device(): whole_rows = lax.all_gather(tokens, ('kv', 'tp'), axis=1, tiled=True)  58.6 us
    all_gather x1, waiting for transfers between devices, half_inputs(): lax.all_gather(activations, ('kv', 'tp'), axis=1, tiled=True)  54.4 us
    reduce_scatter x1, waiting for transfers between devices, per_device(): lax.psum_scatter(jnp.concatenate([jnp.dot(normed, weight_part, preferred_...  42.6 us
    all_gather x1, blocking collectives, per_device(): lax.all_gather(mixed_in, 'kv', axis=0, tiled=True)  30.9 us
    psum x1, blocking collectives, per_device(): squares = lax.psum(jnp.sum(block_float * block_float, axis=1), 'kv')  21.5 us
    unnamed x8, waiting for transfers between devices  19.7 us
  transfers between devices with their start and end apart: 7, of which 7 were waited for; matrix products, arithmetic and copies ran while one was open for 0% of the time, Pallas kernels for 0%

profile of v1, /device:TPU:0, one launch (start us, length us, event | category | flops | bytes accessed | tf_op | source)
XLA Modules:
  0.0 531.4 jit_solution(10207667071552576225)
XLA Ops:
  8.0 58.6 %all-gather.5.cloned.1.call-done = bf16[256,4096]{1,0:T(8,128)(2,1)} async-done(((bf16[256,128]{1,0:T(8,128)(2,1)}), bf16[256,4096]{1,0:T(8,128)(2,1)}) %all-gather.5.cloned.1.call-update) | async-done | bytes 2097168 | tf_op jit(solution)/shard_map/all_gather | solution.py:54
  66.6 2.1 fusion
  68.7 3.4 fusion.12
  72.1 7.5 %convolution_convert_fusion = bf16[256,4096]{1,0:T(8,128)(2,1)} fusion(bf16[352,4096]{1,0:T(8,128)(2,1)S(1)} %copy-done, bf16[4096,352]{0,1:T(8,128)(2,1)} %param.22, bf16[256,4096]{1,0:T(8,128)(2,1)} %all-gather.5.cloned.1.call-done, f32[4096]{0:T(1024)S(1)} %copy-done.9, f32[256,352]{0,1:T(8,128)S(1)} %fusion.12, f32[256]{0:T(256)S(1)} %add_rsqrt_fusion.2), kind=kOutput, calls=%fused_computation.5 | convolution fusion | flops 1481220096 | bytes 10339328 | tf_op jit(solution)/shard_map/dot_general | solution.py:62
  79.7 68.1 %reduce-scatter.7.cloned.1.call-done = bf16[256,512]{1,0:T(8,128)(2,1)} async-done(((bf16[256,4096]{1,0:T(8,128)(2,1)}), bf16[256,512]{1,0:T(8,128)(2,1)}) %reduce-scatter.7.cloned.1.call-update) | async-done | bytes 262160 | tf_op jit(solution)/shard_map/reduce_scatter | solution.py:61
  148.6 16.4 %all-gather.9.cloned.1.call-done = bf16[1024,512]{1,0:T(8,128)(2,1)} async-done(((bf16[256,512]{1,0:T(8,128)(2,1)}), bf16[1024,512]{1,0:T(8,128)(2,1)}) %all-gather.9.cloned.1.call-update) | async-done | bytes 1048592 | tf_op jit(solution)/shard_map/all_gather | solution.py:11
  165.0 1.5 reduce_sum.49
  166.5 1.2 fusion.42
  167.7 1.3 convolution_convert_fusion.3
  169.1 1.3 convolution_convert_fusion.2
  171.1 1.1 pad_maximum_fusion
  172.3 21.5 %psum.7 = f32[256]{0:T(256)S(1)} all-reduce(f32[256]{0:T(256)S(1)} %get-tuple-element.2), channel_id=1, replica_groups=mesh['kv'=8,'tp'=4] {'kv'}, use_global_device_ids=true, to_apply=%region_5.6 | all-reduce | flops 256 | bytes 2048 | tf_op jit(solution)/shard_map/psum | solution.py:82
  193.9 42.6 %reduce-scatter.9.cloned.1.call-done = bf16[32,2048]{1,0:T(8,128)(2,1)} async-done(((bf16[256,2048]{1,0:T(8,128)(2,1)}), bf16[32,2048]{1,0:T(8,128)(2,1)}) %reduce-scatter.9.cloned.1.call-update) | async-done | bytes 131088 | tf_op jit(solution)/shard_map/reduce_scatter | solution.py:86
  241.2 1.5 div.63
  243.6 8.2 %multiply_add_fusion = f32[32,4,128,128]{3,2,1,0:T(8,128)S(1)} fusion(f32[32,4,128,128]{3,2,1,0:T(8,128)} %param.19, f32[32,4,128]{2,1,0:T(4,128)S(1)} %mul.203, f32[32,4,128]{2,1,0:T(4,128)S(1)} %bitcast.41, f32[32,4,128]{2,1,0:T(4,128)S(1)} %bitcast.40), kind=kLoop, calls=%fused_computation | loop fusion | flops 6291456 | bytes 16973824 | tf_op jit(solution)/shard_map/add | solution.py:111
  251.8 7.2 %fusion.65 = f32[32,4,1,128]{3,2,1,0:T(1,128)S(1)} fusion(f32[32,4,128,128]{3,2,1,0:T(8,128)S(1)} %multiply_add_fusion, f32[32,4,128,1]{2,3,1,0:T(1,128)S(1)} %bitcast.39), kind=kOutput, calls=%fused_computation.68 | convolution fusion | flops 25165824 | bytes 8519680 | tf_op jit(solution)/shard_map/bhkv,bhk->bhv/dot_general | solution.py:113
  259.3 30.9 %all_gather.18 = bf16[256,512]{1,0:T(8,128)(2,1)S(1)} all-gather(bf16[32,512]{1,0:T(8,128)(2,1)S(1)} %fusion.61), channel_id=1, replica_groups=mesh['kv'=8,'tp'=4] {'kv'}, dimensions={0}, use_global_device_ids=true | all-gather | bytes 294912 | tf_op jit(solution)/shard_map/all_gather | solution.py:123
  291.4 18.9 %reduce-scatter.13.cloned.1.call-done = bf16[128,256]{1,0:T(8,128)(2,1)} async-done(((bf16[512,256]{1,0:T(8,128)(2,1)}), bf16[128,256]{1,0:T(8,128)(2,1)}) %reduce-scatter.13.cloned.1.call-update) | async-done | bytes 65552
  312.2 54.4 %all-gather.7.cloned.1.call-done = bf16[256,4096]{1,0:T(8,128)(2,1)} async-done(((bf16[256,128]{1,0:T(8,128)(2,1)}), bf16[256,4096]{1,0:T(8,128)(2,1)}) %all-gather.7.cloned.1.call-update) | async-done | bytes 2097168 | tf_op jit(solution)/shard_map/all_gather | solution.py:16
  366.6 2.1 fusion.2
  368.7 3.4 fusion.18
  372.1 8.9 %fusion.37 = f32[256,4096]{1,0:T(8,128)} fusion(bf16[352,4096]{1,0:T(8,128)(2,1)} %param.35, bf16[4096,352]{0,1:T(8,128)(2,1)} %param.34, bf16[256,4096]{1,0:T(8,128)(2,1)} %all-gather.7.cloned.1.call-done, f32[4096]{0:T(1024)S(1)} %copy-done.6, f32[256,352]{0,1:T(8,128)S(1)} %fusion.18, f32[256]{0:T(256)S(1)} %add_rsqrt_fusion.1), kind=kOutput, calls=%fused_computation.27 | convolution fusion | flops 1480171520 | bytes 12436480 | tf_op jit(solution)/shard_map/dot_general | solution.py:27
  381.1 141.9 %reduce-scatter.11.cloned.1.call-done = f32[256,128]{1,0:T(8,128)} async-done(((f32[256,4096]{1,0:T(8,128)}), f32[256,128]{1,0:T(8,128)}) %reduce-scatter.11.cloned.1.call-update) | async-done | bytes 131088 | tf_op jit(solution)/shard_map/reduce_scatter | solution.py:26
  523.0 1.6 add_convert_fusion.1
  (58 shorter events, 11.4 us)
Async XLA Ops:
  7.2 65.0 %copy-start = (bf16[352,4096]{1,0:T(8,128)(2,1)S(1)}, bf16[352,4096]{1,0:T(8,128)(2,1)}, u32[]{:S(2)}) copy-start(bf16[352,4096]{1,0:T(8,128)(2,1)} %param.23) | copy-start | bytes 8650756
  7.2 59.4 %all-gather.5.cloned.1.call-start = ((), (), s32[]{:S(2)}) async-start(), calls=%async_computation.4 | async-start | bytes 2162688 | tf_op jit(solution)/shard_map/all_gather | solution.py:54
  7.9 139.8 %reduce-scatter.7.cloned.1.call-start = ((), (), s32[]{:S(2)}) async-start(), calls=%async_computation.5 | async-start | bytes 2359296 | tf_op jit(solution)/shard_map/reduce_scatter | solution.py:61
  68.7 3.5 copy-start.9
  79.6 85.4 %all-gather.9.cloned.1.call-start = ((), (), s32[]{:S(2)}) async-start(), calls=%async_computation.9 | async-start | bytes 1310720 | tf_op jit(solution)/shard_map/all_gather | solution.py:11
  147.8 88.7 %reduce-scatter.9.cloned.1.call-start = ((), (), s32[]{:S(2)}) async-start(), calls=%async_computation.6 | async-start | bytes 1179648 | tf_op jit(solution)/shard_map/reduce_scatter | solution.py:86
  166.5 4.0 copy-start.3
  166.5 4.3 copy-start.4
  170.4 1.8 copy-start.7
  172.2 138.1 %reduce-scatter.13.cloned.1.call-start = ((), (), s32[]{:S(2)}) async-start(), calls=%async_computation.10 | async-start | bytes 327680
  251.8 7.2 %copy-start.1 = (f32[32,4,128,128]{3,2,1,0:T(8,128)}, f32[32,4,128,128]{3,2,1,0:T(8,128)S(1)}, u32[]{:S(2)}) copy-start(f32[32,4,128,128]{3,2,1,0:T(8,128)S(1)} %multiply_add_fusion) | copy-start | bytes 25165828
  251.8 7.3 %copy-start.8 = (f32[128]{0:T(128)S(1)}, f32[128]{0:T(128)}, u32[]{:S(2)}) copy-start(f32[128]{0:T(128)} %param.30) | copy-start | bytes 1540
  251.8 38.4 %copy-start.5 = (bf16[512,512]{1,0:T(8,128)(2,1)S(1)}, bf16[512,512]{1,0:T(8,128)(2,1)}, u32[]{:S(2)}) copy-start(bf16[512,512]{1,0:T(8,128)(2,1)} %param.31) | copy-start | bytes 1572868
  259.0 109.7 %copy-start.6 = (f32[4096]{0:T(1024)S(1)}, f32[4096]{0:T(1024)}, u32[]{:S(2)}) copy-start(f32[4096]{0:T(1024)} %param.32) | copy-start | bytes 49156
  291.3 75.3 %all-gather.7.cloned.1.call-start = ((), (), s32[]{:S(2)}) async-start(), calls=%async_computation.7 | async-start | bytes 2162688 | tf_op jit(solution)/shard_map/all_gather | solution.py:16
  311.9 211.1 %reduce-scatter.11.cloned.1.call-start = ((), (), s32[]{:S(2)}) async-start(), calls=%async_computation.8 | async-start | bytes 4325376 | tf_op jit(solution)/shard_map/reduce_scatter | solution.py:26
  381.1 141.9 %copy-start.2 = (bf16[256,128]{1,0:T(8,128)(2,1)S(1)}, bf16[256,128]{1,0:T(8,128)(2,1)}, u32[]{:S(2)}) copy-start(bf16[256,128]{1,0:T(8,128)(2,1)} %add_convert_fusion.2) | copy-start | bytes 196612
Sparse Core Ops, SparseCore 0:
  10.8 55.6 all-gather.4
  79.7 67.9 reduce-scatter.6
  149.3 15.6 all-gather.8
  172.3 64.0 reduce-scatter.8
  291.5 18.7 reduce-scatter.12
  313.6 52.9 all-gather.6
  381.2 141.7 reduce-scatter.10
